TPU v7x, 32 devices: a whole 2x2x4 slice. The times are simulated.
32 devices in a mesh: sp: 8 (over z, y), tp: 4 (over x, core).
Axes of the slice: x: 2, y: 2, z: 4, core: 2. Of those that a mesh axis runs over, the one named last changes fastest.
Arguments:
- mixer_input: bfloat16 [4096, 1024], P('sp', 'tp'), may hold values from -6 to 6
- residual: bfloat16 [4096, 2048], P(('sp', 'tp')), may hold values from -6 to 6
- decay_real: float32 [64, 64], P('tp'), may hold values from -0.07 to 0
- decay_imag: float32 [64, 64], P('tp'), may hold values from 0.3 to 3
- log_step: float32 [64], P('tp'), may hold values from -0.7 to 0.7
- input_re: float32 [64, 64, 16], P('tp'), may hold values from -1.5 to 1.5
- input_im: float32 [64, 64, 16], P('tp'), may hold values from -1.5 to 1.5
- output_re: float32 [64, 16, 64], P('tp'), may hold values from -0.5 to 0.5
- output_im: float32 [64, 16, 64], P('tp'), may hold values from -0.5 to 0.5
- skip_gain: float32 [64, 16], P('tp'), may hold values from -4 to 4
- glu_weight: bfloat16 [1024, 1024], replicated, may hold values from -0.1875 to 0.1875
- glu_bias: float32 [1024], replicated, may hold values from -4 to 4
- mix_gain: float32 [1024], replicated, may hold values from 0.1 to 1.9
- out_weight: bfloat16 [1024, 2048], replicated, may hold values from -0.1875 to 0.1875
- norm_gain: float32 [2048], replicated, may hold values from 0.1 to 1.9
- route_ids: int32 [4096, 4], P(('sp', 'tp')), may hold values from 0 to 31, all different within a row; in each aligned block of 128 rows (0 to 127, 128 to 255, ...) at most 24 rows name the same one
- route_gates: float32 [4096, 4], P(('sp', 'tp')), may hold values from 0.25 to 1
- expert_gate: bfloat16 [32, 2048, 512], P(('sp', 'tp')), may hold values from -0.125 to 0.125
- expert_up: bfloat16 [32, 2048, 512], P(('sp', 'tp')), may hold values from -0.125 to 0.125
- expert_down: bfloat16 [32, 512, 2048], P(('sp', 'tp')), may hold values from -0.25 to 0.25
- shared_gate: bfloat16 [2048, 512], replicated, may hold values from -0.125 to 0.125
- shared_up: bfloat16 [2048, 512], replicated, may hold values from -0.125 to 0.125
- shared_down: bfloat16 [512, 2048], replicated, may hold values from -0.25 to 0.25
Outputs:
- layer_out: bfloat16 [4096, 2048], P(('sp', 'tp'))
Inputs may be any that keep to these rules, and one draw needn't show every extreme that they name: `route_ids`: each row names 4 different experts; among the 128 rows of one device no expert is named by more than 24 rows, and in every draw some expert is named by exactly 24 of them.
All inputs are finite; a program needn't handle non-finite values.
Results may differ from a plain program's by a relative error of at most 0.018.
Values may be sent and summed in bfloat16 or wider, within the bound.
A program may use at most 128 MiB of HBM per device.

v0:
```python
import functools
import math

import jax
import jax.numpy as jnp
from jax import lax
from jax.experimental import pallas as pl
from jax.experimental.pallas import tpu as pltpu
from jax.sharding import PartitionSpec as P

NORM_EPS = 1e-06
HIGHEST = lax.Precision.HIGHEST
MESH = pl.DeviceIdType.MESH


def exchange_kernel(count, position, member, same, block_ref, out_ref, send_sem, recv_sem, own_sem):
    me = position()
    barrier = pltpu.get_barrier_semaphore()

    def greet(step, carry):
        pl.semaphore_signal(
            barrier, inc=1, device_id=member(lax.rem(me + step, count)), device_id_type=MESH
        )
        return carry

    def copy(step):
        to = lax.rem(me + step, count)
        return pltpu.make_async_remote_copy(
            src_ref=block_ref if same else block_ref.at[to],
            dst_ref=out_ref.at[me],
            send_sem=send_sem.at[step],
            recv_sem=recv_sem.at[step],
            device_id=member(to),
            device_id_type=MESH,
        )

    def begin(step, carry):
        copy(step).start()
        return carry

    def finish(step, carry):
        copy(step).wait()
        return carry

    own = pltpu.make_async_copy(block_ref if same else block_ref.at[me], out_ref.at[me], own_sem)
    own.start()
    lax.fori_loop(1, count, greet, 0)
    pl.semaphore_wait(barrier, count - 1)
    lax.fori_loop(1, count, begin, 0)
    lax.fori_loop(1, count, finish, 0)
    own.wait()


def exchange(block, count, position, member, collective_id, same=False):
    shape = (count,) + block.shape if same else block.shape
    return pl.pallas_call(
        functools.partial(exchange_kernel, count, position, member, same),
        out_shape=jax.ShapeDtypeStruct(shape, block.dtype),
        in_specs=[pl.BlockSpec(memory_space=pl.ANY)],
        out_specs=pl.BlockSpec(memory_space=pl.ANY),
        scratch_shapes=[
            pltpu.SemaphoreType.DMA((count,)),
            pltpu.SemaphoreType.DMA((count,)),
            pltpu.SemaphoreType.DMA,
        ],
        compiler_params=pltpu.CompilerParams(collective_id=collective_id, has_side_effects=True),
    )(block)


def gather_sp(block):
    return exchange(
        block,
        lax.axis_size("sp"),
        lambda: lax.axis_index("sp"),
        lambda index: (index, lax.axis_index("tp")),
        1,
        same=True,
    )


def exchange_tp(block):
    return exchange(
        block,
        lax.axis_size("tp"),
        lambda: lax.axis_index("tp"),
        lambda index: (lax.axis_index("sp"), index),
        2,
    )


def exchange_all(block, collective_id):
    width = lax.axis_size("tp")
    return exchange(
        block,
        lax.axis_size(("sp", "tp")),
        lambda: lax.axis_index("sp") * width + lax.axis_index("tp"),
        lambda index: (index // width, lax.rem(index, width)),
        collective_id,
    )


CHUNK = 16


def times(a, b):
    return (a[0] * b[0] - a[1] * b[1], a[0] * b[1] + a[1] * b[0])


def mixer(inputs, decay_real, decay_imag, log_step, input_re, input_im, output_re, output_im, skip):
    length = inputs.shape[0]
    groups, states, channels = input_re.shape
    chunks = length // CHUNK
    step_size = jnp.exp(log_step)[:, None]
    log_rate = decay_real * step_size
    turn_angle = decay_imag * step_size

    def powers(count):
        magnitude = jnp.exp(count * log_rate)
        return (magnitude * jnp.cos(count * turn_angle), magnitude * jnp.sin(count * turn_angle))

    bar_re, bar_im = powers(1.0)
    denominator = decay_real * decay_real + decay_imag * decay_imag
    less_one = bar_re - 1.0
    coef = (
        (less_one * decay_real + bar_im * decay_imag) / denominator,
        (bar_im * decay_real - less_one * decay_imag) / denominator,
    )
    drive = times((coef[0][:, :, None], coef[1][:, :, None]), (input_re, input_im))
    steps = jnp.arange(1, CHUNK + 1, dtype=jnp.float32)
    ahead = powers(steps[:, None, None])
    ahead = tuple(jnp.swapaxes(part, 0, 1)[:, :, None, :] for part in ahead)
    reads = times(ahead, (output_re[:, None], output_im[:, None]))
    reads = jnp.concatenate([reads[0], -reads[1]], axis=3).reshape(
        groups, CHUNK * channels, 2 * states
    )
    back = powers(-steps[:, None, None])
    back = tuple(jnp.swapaxes(part, 0, 1)[:, :, None, :] for part in back)
    drive = tuple(jnp.swapaxes(part, 1, 2)[:, None] for part in drive)
    feeds = times(back, drive)
    feeds = jnp.concatenate(feeds, axis=3).reshape(groups, CHUNK * channels, 2 * states)
    rows = jnp.arange(CHUNK * channels, dtype=jnp.int32) // channels
    kernel = jnp.einsum("gsn,gtn->gst", feeds, reads, precision=HIGHEST)
    kernel = jnp.where(rows[:, None] <= rows[None, :], kernel, 0.0)
    wide = (
        inputs.reshape(chunks, CHUNK, groups, channels)
        .transpose(2, 0, 1, 3)
        .reshape(groups, chunks, CHUNK * channels)
        .astype(jnp.float32)
    )
    local = jnp.einsum("gks,gst->gkt", wide, kernel, precision=HIGHEST)
    driven = jnp.einsum("gks,gsn->gkn", wide, feeds, precision=HIGHEST)
    whole = tuple(part[:, None] for part in powers(float(CHUNK)))
    state = times(whole, (driven[:, :, :states], driven[:, :, states:]))
    offset = 1
    while offset < chunks:
        prior = tuple(
            jnp.pad(part[:, :-offset], ((0, 0), (offset, 0), (0, 0))) for part in state
        )
        moved = times(tuple(part[:, None] for part in powers(float(CHUNK * offset))), prior)
        state = (state[0] + moved[0], state[1] + moved[1])
        offset *= 2
    ends = jnp.concatenate([state[0][:, -1], state[1][:, -1]], axis=1)
    ends = ends.reshape(groups * states * 2 // 128, 128)
    pieces = gather_sp(ends).reshape(-1, groups, 2 * states)
    my_index = lax.axis_index("sp")
    sources = jnp.arange(pieces.shape[0], dtype=jnp.int32)
    earlier = sources < my_index
    distance = jnp.where(earlier, my_index - 1 - sources, 0).astype(jnp.float32)[:, None, None]
    weight = jnp.where(earlier, 1.0, 0.0).astype(jnp.float32)[:, None, None]
    block_angle = jnp.mod(float(length) * turn_angle, 2.0 * math.pi)
    magnitude = jnp.exp(distance * (float(length) * log_rate)) * weight
    factor = (
        magnitude * jnp.cos(distance * block_angle),
        magnitude * jnp.sin(distance * block_angle),
    )
    added = times(factor, (pieces[:, :, :states], pieces[:, :, states:]))
    carried = tuple(jnp.sum(part, axis=0)[:, None] for part in added)
    starts = powers(float(CHUNK) * jnp.arange(chunks, dtype=jnp.float32)[:, None, None])
    starts = tuple(jnp.swapaxes(part, 0, 1) for part in starts)
    carried = times(starts, carried)
    before = jnp.concatenate(
        [
            jnp.pad(state[i][:, :-1], ((0, 0), (1, 0), (0, 0))) + carried[i]
            for i in range(2)
        ],
        axis=2,
    )
    readout = local + jnp.einsum("gkn,gtn->gkt", before, reads, precision=HIGHEST)
    gains = jnp.broadcast_to(skip[:, None, :], (groups, CHUNK, channels))
    mixed = jax.nn.gelu(readout + gains.reshape(groups, 1, -1) * wide).astype(jnp.bfloat16)
    return (
        mixed.reshape(groups, chunks, CHUNK, channels)
        .transpose(1, 2, 0, 3)
        .reshape(length, groups * channels)
    )


def rms_scale(values, gain):
    return values * lax.rsqrt(jnp.mean(values * values, axis=-1, keepdims=True) + NORM_EPS) * gain


def earlier_rows(onehot):
    count = onehot.shape[0]
    lower = jnp.tril(jnp.ones((count, count), jnp.bfloat16))
    return jnp.dot(lower, onehot.astype(jnp.bfloat16), preferred_element_type=jnp.float32)


def expert_apply(arrived, gate_w, up_w, down_w):
    block_shape = arrived.shape
    flattened = arrived.reshape(-1, block_shape[-1])
    hidden = (
        jax.nn.silu(jnp.dot(flattened, gate_w, preferred_element_type=jnp.float32))
        * jnp.dot(flattened, up_w, preferred_element_type=jnp.float32)
    ).astype(jnp.bfloat16)
    result = jnp.dot(hidden, down_w, preferred_element_type=jnp.float32).astype(jnp.bfloat16)
    return result.reshape(block_shape)


def on_device(
    mixer_input,
    residual,
    decay_real,
    decay_imag,
    log_step,
    input_re,
    input_im,
    output_re,
    output_im,
    skip_gain,
    glu_weight,
    glu_bias,
    mix_gain,
    out_weight,
    norm_gain,
    route_ids,
    route_gates,
    expert_gate,
    expert_up,
    expert_down,
    shared_gate,
    shared_up,
    shared_down,
):
    mixed = mixer(
        mixer_input,
        decay_real,
        decay_imag,
        log_step,
        input_re,
        input_im,
        output_re,
        output_im,
        skip_gain,
    )
    tp_count = lax.axis_size("tp")
    token_rows = exchange_tp(mixed.reshape(tp_count, -1, mixed.shape[1]))
    token_rows = token_rows.transpose(1, 0, 2).reshape(token_rows.shape[1], -1)
    pre_gate = jnp.dot(token_rows, glu_weight, preferred_element_type=jnp.float32) + glu_bias
    gated = token_rows.astype(jnp.float32) * jax.nn.sigmoid(pre_gate)
    normed = rms_scale(gated, mix_gain).astype(jnp.bfloat16)
    stream = residual.astype(jnp.float32) + jnp.dot(
        normed, out_weight, preferred_element_type=jnp.float32
    )
    hidden_in = rms_scale(stream, norm_gain).astype(jnp.bfloat16)
    shared_hidden = (
        jax.nn.silu(jnp.dot(hidden_in, shared_gate, preferred_element_type=jnp.float32))
        * jnp.dot(hidden_in, shared_up, preferred_element_type=jnp.float32)
    ).astype(jnp.bfloat16)
    total = stream + jnp.dot(shared_hidden, shared_down, preferred_element_type=jnp.float32)
    row_count, top_count = route_ids.shape
    model_width = hidden_in.shape[1]
    expert_count = lax.axis_size(("sp", "tp"))
    capacity = max(2, 3 * row_count * top_count // (2 * expert_count))
    flat_ids = route_ids.reshape(-1)
    onehot = (flat_ids[:, None] == jnp.arange(expert_count, dtype=jnp.int32)[None, :]).astype(
        jnp.float32
    )
    ranks = jnp.sum((earlier_rows(onehot) - onehot) * onehot, axis=1)
    slots = (flat_ids * capacity + ranks.astype(jnp.int32)).reshape(row_count, top_count)
    slot_numbers = jnp.arange(expert_count * capacity, dtype=jnp.int32)
    hits = [slots[:, index : index + 1] == slot_numbers for index in range(top_count)]
    placed = functools.reduce(jnp.logical_or, hits).astype(jnp.bfloat16)
    outgoing = (
        lax.dot_general(
            placed, hidden_in, (((0,), (0,)), ((), ())), preferred_element_type=jnp.float32
        )
        .astype(jnp.bfloat16)
        .reshape(expert_count, capacity, model_width)
    )
    gates = sum(
        jnp.where(hits[index], route_gates[:, index : index + 1], 0.0)
        for index in range(top_count)
    )
    coarse = gates.astype(jnp.bfloat16)
    fine = (gates - coarse.astype(jnp.float32)).astype(jnp.bfloat16)
    gate_w = expert_gate[0]
    up_w = expert_up[0]
    down_w = expert_down[0]
    returned = exchange_all(
        expert_apply(exchange_all(outgoing, 3), gate_w, up_w, down_w), 4
    )
    rows = returned.reshape(expert_count * capacity, model_width)
    total = (
        total
        + jnp.dot(coarse, rows, preferred_element_type=jnp.float32)
        + jnp.dot(fine, rows, preferred_element_type=jnp.float32)
    )
    return total.astype(jnp.bfloat16)


def solution(mesh):
    return jax.shard_map(
        on_device,
        mesh=mesh,
        in_specs=(
            P("sp", "tp"),
            P(("sp", "tp"), None),
            P("tp", None),
            P("tp", None),
            P("tp"),
            P("tp", None, None),
            P("tp", None, None),
            P("tp", None, None),
            P("tp", None, None),
            P("tp", None),
            P(),
            P(),
            P(),
            P(),
            P(),
            P(("sp", "tp"), None),
            P(("sp", "tp"), None),
            P(("sp", "tp"), None, None),
            P(("sp", "tp"), None, None),
            P(("sp", "tp"), None, None),
            P(),
            P(),
            P(),
        ),
        out_specs=P(("sp", "tp"), None),
        check_vma=False,
    )
```

profile of v0, /device:TPU:15, one launch (start us, length us, event | category | flops | bytes accessed | tf_op | source)
XLA Modules:
  0.0 262.3 jit_solution(5140108026339101928)
XLA Ops:
  0.0 0.0 copy-start
  0.0 0.8 exp.65
  0.8 1.0 cosine_multiply_fusion
  1.8 1.0 fusion.90
  2.9 1.0 subtract_bitcast_fusion
  3.9 0.0 copy-start.8
  3.9 5.1 %multiply_subtract_fusion = (f32[16,16,16,64]{3,2,1,0:T(8,128)}, f32[16,16,16,64]{3,2,1,0:T(8,128)}, f32[16,16,16,64]{3,2,1,0:T(8,128)}, f32[16,16,16,64]{3,2,1,0:T(8,128)}) fusion(f32[16,16,64]{2,1,0:T(8,128)} %param.31, f32[16,16,64]{2,1,0:T(8,128)S(1)} %get-tuple-element.43, f32[16,16,64]{2,1,0:T(8,128)} %param.30, ...), kind=kLoop, calls=%fused_computation.18 | loop fusion | flops 3407872 | bytes 4718592 | tf_op jit(solution)/shard_map/sub | solution.py:106
  9.0 0.0 copy-done.8
  9.0 2.4 reshape.173
  11.4 3.3 %copy.54 = bf16[16,32,16,16]{1,3,2,0:T(8,128)(2,1)S(1)} copy(bf16[16,32,16,16]{3,0,2,1:T(8,128)(2,1)} %bitcast.93) | data formatting | bytes 524288 | tf_op jit(solution)/shard_map/transpose | solution.py:146
  14.7 3.9 %fusion.34 = f32[16,128,32]{1,2,0:T(8,128)S(1)} fusion(bf16[16,32,256]{1,2,0:T(8,128)(2,1)S(1)} %bitcast.87, f32[16,256,64]{2,1,0:T(8,128)} %bitcast.83, f32[16,256,64]{2,1,0:T(8,128)} %bitcast.85), kind=kOutput, calls=%fused_computation.44 | convolution fusion | flops 201850880 | bytes 2621440 | tf_op jit(solution)/shard_map/gks,gsn->gkn/dot_general | solution.py:151
  18.5 0.2 copy.71
  18.7 0.1 multiply_subtract_fusion.2
  18.9 0.1 subtract_add_fusion.2
  19.1 0.1 subtract_add_fusion.1
  19.2 0.1 fusion.54
  19.4 0.1 fusion.58
  19.5 0.1 fusion.62
  19.6 0.7 slice.116
  20.3 0.7 pad_maximum_fusion.7.block_ref
  20.9 6.3 %shard_map.217 = f32[8,16,128]{2,1,0:T(8,128)} custom-call(f32[16,128]{1,0:T(8,128)} %pad_maximum_fusion.7.block_ref), custom_call_target="tpu_custom_call" | custom-call | tf_op jit(solution)/shard_map/pallas_call | solution.py:56
  27.3 0.0 copy-start.1
  27.3 1.4 subtract_reduce_fusion
  28.7 2.3 subtract_add_fusion
  31.1 0.1 pad_maximum_fusion.6
  31.2 0.0 copy-done.1
  31.2 0.0 copy-start.2
  31.2 0.0 copy-start.3
  31.2 5.0 %fusion.32 = f32[16,32,256]{2,1,0:T(8,128)} fusion(f32[16,256,64]{2,1,0:T(8,128)} %bitcast.81, f32[16,256,64]{2,1,0:T(8,128)S(1)} %bitcast.79, f32[16,32,128]{2,0,1:T(8,128)S(1)} %pad_maximum_fusion.6), kind=kOutput, calls=%fused_computation.42 | convolution fusion | flops 201850880 | bytes 2883584 | tf_op jit(solution)/shard_map/gkn,gtn->gkt/dot_general | solution.py:188
  36.2 0.0 copy-done.2
  36.2 0.0 copy-done.3
  36.2 7.7 %fusion.33 = f32[16,256,256]{2,1,0:T(8,128)} fusion(f32[16,256,64]{2,1,0:T(8,128)S(1)} %bitcast.82, f32[16,256,64]{2,1,0:T(8,128)S(1)} %bitcast.80, f32[16,256,64]{2,1,0:T(8,128)S(1)} %bitcast.84, f32[16,256,64]{2,1,0:T(8,128)} %bitcast.86), kind=kOutput, calls=%fused_computation.43 | convolution fusion | flops 1611661312 | bytes 8388608 | tf_op jit(solution)/shard_map/gsn,gtn->gst/dot_general | solution.py:142
  44.0 0.7 broadcast_compare_fusion
  44.7 0.3 copy.59
  45.0 0.0 copy-done.10
  45.1 0.1 mul.908
  45.2 5.1 %fusion.44 = bf16[16,32,256]{2,1,0:T(8,128)(2,1)} fusion(f32[16,32,256]{2,1,0:T(8,128)} %fusion.32, bf16[16,32,256]{1,2,0:T(8,128)(2,1)S(1)} %bitcast.89, f32[16,256,256]{2,1,0:T(8,128)} %fusion.33, pred[256,256]{1,0:T(8,128)(4,1)} %broadcast_compare_fusion, bf16[16,32,256]{2,1,0:T(8,128)(2,1)S(1)} %copy.59, f32[16,256]{1,0:T(8,128)S(1)} %mul.908), kind=kOutput, calls=%fused_computation.52 | convolution fusion | flops 405405696 | bytes 5586944 | tf_op jit(solution)/shard_map/gks,gst->gkt/dot_general | solution.py:150
  50.3 1.4 copy.60
  51.8 4.2 %copy.61 = bf16[32,16,16,16]{3,2,1,0:T(8,128)(2,1)} copy(bf16[32,16,16,16]{0,3,1,2:T(8,128)(2,1)S(1)} %bitcast.94) | data formatting | bytes 524288 | tf_op jit(solution)/shard_map/transpose | solution.py:193
  55.9 3.9 %reshape_reshape.3.block_ref = bf16[4,128,256]{2,1,0:T(8,128)(2,1)} reshape(bf16[32,16,16,16]{3,2,1,0:T(8,128)(2,1)} %copy.61) | data formatting | bytes 524288 | tf_op jit(solution)/shard_map/reshape;reshape | solution.py:256
  59.8 7.0 %shard_map.218 = bf16[4,128,256]{2,1,0:T(8,128)(2,1)} custom-call(bf16[4,128,256]{2,1,0:T(8,128)(2,1)} %reshape_reshape.3.block_ref), custom_call_target="tpu_custom_call" | custom-call | tf_op jit(solution)/shard_map/pallas_call | solution.py:56
  66.9 1.1 copy.62
  68.0 0.1 copy.63
  68.1 0.0 copy-start.5
  68.2 0.0 copy-start.12
  68.2 2.4 multiply_reduce_fusion.1
  70.6 0.4 copy-done.5
  71.0 0.0 copy-done.12
  71.0 2.2 multiply_reduce_fusion
  73.2 0.5 fusion.113
  73.7 0.0 copy-start.11
  73.7 4.1 %convolution_add_fusion.2 = f32[128,2048]{1,0:T(8,128)} fusion(f32[128,2048]{1,0:T(8,128)S(1)} %get-tuple-element.60, bf16[512,2048]{1,0:T(8,128)(2,1)} %param.45, bf16[2048,512]{1,0:T(8,128)(2,1)} %param.44, f32[128,512]{1,0:T(8,128)S(1)} %fusion.113, f32[2048]{0:T(1024)S(1)} %copy-done.9, f32[128]{0:T(128)S(1)} %add_rsqrt_fusion), kind=kOutput, calls=%fused_computation.6 | convolution fusion | flops 538312704 | bytes 6562304 | tf_op jit(solution)/shard_map/dot_general | solution.py:269
  77.8 0.1 copy.64
  78.0 0.1 eq.75
  78.1 0.3 fusion.28
  78.4 0.1 convert_element_type.91
  78.5 0.1 copy.65
  78.6 2.9 %convolution_convert_fusion.1 = bf16[768,2048]{1,0:T(8,128)(2,1)} fusion(s32[128]{0:T(128)S(1)} %get-tuple-element.54, s32[128]{0:T(128)S(1)} %get-tuple-element.55, s32[128]{0:T(128)S(1)} %get-tuple-element.56, s32[128]{0:T(128)S(1)} %get-tuple-element.53, f32[128,2048]{1,0:T(8,128)S(1)} %get-tuple-element.60, f32[2048]{0:T(1024)S(1)} %copy-done.9, ...), kind=kOutput, calls=%fused_computation.3 | convolution fusion | flops 405700608 | bytes 4205056 | tf_op jit(solution)/shard_map/dot_general | solution.py:284
  81.5 82.7 %shard_map.219 = bf16[32,24,2048]{2,1,0:T(8,128)(2,1)} custom-call(bf16[32,24,2048]{2,1,0:T(8,128)(2,1)} %bitcast.92), custom_call_target="tpu_custom_call" | custom-call | tf_op jit(solution)/shard_map/pallas_call | solution.py:56
  164.2 5.5 %fusion.6 = f32[768,512]{1,0:T(8,128)} fusion(bf16[768,2048]{1,0:T(8,128)(2,1)} %bitcast.95, bf16[1,2048,512]{2,1,0:T(8,128)(2,1)} %param.40), kind=kOutput, calls=%fused_computation.14 | convolution fusion | flops 1610612736 | bytes 6815744 | tf_op jit(solution)/shard_map/dot_general | solution.py:212
  169.7 8.2 %convolution_convert_fusion = bf16[768,2048]{1,0:T(8,128)(2,1)} fusion(bf16[1,512,2048]{2,1,0:T(8,128)(2,1)S(1)} %copy-done, f32[768,512]{1,0:T(8,128)} %fusion.6, bf16[768,2048]{1,0:T(8,128)(2,1)} %bitcast.96, bf16[1,2048,512]{2,1,0:T(8,128)(2,1)} %param.41), kind=kOutput, calls=%fused_computation.2 | convolution fusion | flops 3225157632 | bytes 12058624 | tf_op jit(solution)/shard_map/dot_general | solution.py:215
  177.8 80.0 %shard_map.220 = bf16[32,24,2048]{2,1,0:T(8,128)(2,1)} custom-call(bf16[32,24,2048]{2,1,0:T(8,128)(2,1)} %bitcast.97), custom_call_target="tpu_custom_call" | custom-call | tf_op jit(solution)/shard_map/pallas_call | solution.py:56
  257.9 2.8 %convolution_add_fusion.1 = f32[128,2048]{1,0:T(8,128)S(1)} fusion(f32[128,2048]{1,0:T(8,128)S(1)} %copy-done.6, bf16[768,2048]{1,0:T(8,128)(2,1)} %bitcast.90, f32[128]{0:T(128)S(1)} %get-tuple-element.51, s32[128]{0:T(128)S(1)} %get-tuple-element.54, f32[128]{0:T(128)S(1)} %get-tuple-element.52, s32[128]{0:T(128)S(1)} %get-tuple-element.55, ...), kind=kOutput, calls=%fused_computation.5 | convolution fusion | flops 404094976 | bytes 5246976 | tf_op jit(solution)/shard_map/dot_general | solution.py:305
  260.7 1.6 fusion.2
  (41 shorter events, 0.3 us)
Async XLA Ops:
  0.0 169.7 %copy-start = (bf16[1,512,2048]{2,1,0:T(8,128)(2,1)S(1)}, bf16[1,512,2048]{2,1,0:T(8,128)(2,1)}, u32[]{:S(2)}) copy-start(bf16[1,512,2048]{2,1,0:T(8,128)(2,1)} %param.42) | copy-start | bytes 6291460
  3.9 5.1 %copy-start.8 = (bf16[512,256]{1,0:T(8,128)(2,1)S(1)}, bf16[512,256]{1,0:T(8,128)(2,1)}, u32[]{:S(2)}) copy-start(bf16[512,256]{1,0:T(8,128)(2,1)} %param.23) | copy-start | bytes 786436
  27.3 3.9 %copy-start.1 = (f32[16,16,16,64]{3,2,1,0:T(8,128)S(1)}, f32[16,16,16,64]{3,2,1,0:T(8,128)}, u32[]{:S(2)}) copy-start(f32[16,16,16,64]{3,2,1,0:T(8,128)} %get-tuple-element.11) | copy-start | bytes 3145732
  31.2 5.0 %copy-start.2 = (f32[16,16,16,64]{3,2,1,0:T(8,128)S(1)}, f32[16,16,16,64]{3,2,1,0:T(8,128)}, u32[]{:S(2)}) copy-start(f32[16,16,16,64]{3,2,1,0:T(8,128)} %get-tuple-element.12) | copy-start | bytes 3145732
  31.2 5.0 %copy-start.3 = (f32[16,16,16,64]{3,2,1,0:T(8,128)S(1)}, f32[16,16,16,64]{3,2,1,0:T(8,128)}, u32[]{:S(2)}) copy-start(f32[16,16,16,64]{3,2,1,0:T(8,128)} %get-tuple-element.61) | copy-start | bytes 3145732
  36.2 8.8 %copy-start.10 = (f32[16,16]{1,0:T(8,128)S(1)}, f32[16,16]{1,0:T(8,128)}, u32[]{:S(2)}) copy-start(f32[16,16]{1,0:T(8,128)} %param.32) | copy-start | bytes 3076
  55.9 12.2 %copy-start.14 = (f32[1024]{0:T(1024)S(1)}, f32[1024]{0:T(1024)}, u32[]{:S(2)}) copy-start(f32[1024]{0:T(1024)} %param.34) | copy-start | bytes 12292
  68.1 2.8 %copy-start.5 = (bf16[1024,2048]{1,0:T(8,128)(2,1)S(1)}, bf16[1024,2048]{1,0:T(8,128)(2,1)}, u32[]{:S(2)}) copy-start(bf16[1024,2048]{1,0:T(8,128)(2,1)} %param.36) | copy-start | bytes 12582916
  68.2 2.8 %copy-start.12 = (f32[1024]{0:T(1024)S(1)}, f32[1024]{0:T(1024)}, u32[]{:S(2)}) copy-start(f32[1024]{0:T(1024)} %param.35) | copy-start | bytes 12292
  71.0 2.2 copy-start.7
  71.0 2.2 copy-start.9
  73.7 4.2 %copy-start.11 = (s32[128,4]{0,1:T(4,128)S(1)}, s32[128,4]{0,1:T(4,128)}, u32[]{:S(2)}) copy-start(s32[128,4]{0,1:T(4,128)} %param.38) | copy-start | bytes 6148
  177.8 80.0 %copy-start.13 = (f32[128,4]{0,1:T(4,128)S(1)}, f32[128,4]{0,1:T(4,128)}, u32[]{:S(2)}) copy-start(f32[128,4]{0,1:T(4,128)} %param.39) | copy-start | bytes 6148
  177.8 80.0 %copy-start.6 = (f32[128,2048]{1,0:T(8,128)S(1)}, f32[128,2048]{1,0:T(8,128)}, u32[]{:S(2)}) copy-start(f32[128,2048]{1,0:T(8,128)} %convolution_add_fusion.2) | copy-start | bytes 3145732
  257.9 2.9 %copy-start.4 = (bf16[32,24,2048]{2,1,0:T(8,128)(2,1)S(1)}, bf16[32,24,2048]{2,1,0:T(8,128)(2,1)}, u32[]{:S(2)}) copy-start(bf16[32,24,2048]{2,1,0:T(8,128)(2,1)} %shard_map.220) | copy-start | bytes 9437188
where the time goes:
time: 263 us; the launch traced here: 262 us
  Pallas kernels  176 us (67%)
  matrix products  52.2 us (20%)
  local copies, waits for them, and re-layouts  19.6 us (7%)
  other arithmetic  14 us (5%)
    pallas_call x4, Pallas kernels, exchange(): pl.pallas_call(functools.partial(exchange_kernel, count, position, member...  176 us
    dot_general x1, matrix products, expert_apply(): jnp.dot(hidden, down_w, preferred_element_type=jnp.float32)  8.15 us
    dot_general x1, matrix products, mixer(): kernel = jnp.einsum('gsn,gtn->gst', feeds, reads, precision=HIGHEST)  7.74 us
    dot_general x1, matrix products, expert_apply(): jnp.dot(flattened, gate_w, preferred_element_type=jnp.float32)  5.47 us
    sub x2, other arithmetic, times(): return (a[0] * b[0] - a[1] * b[1], a[0] * b[1] + a[1] * b[0])  5.26 us

commit v1 on v0

--- a/solution.py
+++ b/solution.py
@@ -23,8 +23,11 @@
         )
         return carry
 
+    stride = 7 if math.gcd(7, count - 1) == 1 else 1
+
     def copy(step):
-        to = lax.rem(me + step, count)
+        ahead = 1 + lax.rem((step - 1) * stride + count // 4, count - 1)
+        to = lax.rem(me + ahead, count)
         return pltpu.make_async_remote_copy(
             src_ref=block_ref if same else block_ref.at[to],
             dst_ref=out_ref.at[me],

time: 263 us -> 249 us (0.947)
  Pallas kernels: 176 us -> 161 us
    pallas_call x4, Pallas kernels: 176 us -> 161 us  [exchange(): pl.pallas_call(functools.partial(exchange_kernel, count, position, member...]
where the time goes in v1:
time: 249 us; the launch traced here: 247 us
  Pallas kernels  161 us (65%)
  matrix products  52.2 us (21%)
  local copies, waits for them, and re-layouts  19.6 us (8%)
  other arithmetic  14 us (6%)
    pallas_call x4, Pallas kernels, exchange(): pl.pallas_call(functools.partial(exchange_kernel, count, position, member...  161 us
    dot_general x1, matrix products, expert_apply(): jnp.dot(hidden, down_w, preferred_element_type=jnp.float32)  8.15 us
    dot_general x1, matrix products, mixer(): kernel = jnp.einsum('gsn,gtn->gst', feeds, reads, precision=HIGHEST)  7.74 us
    dot_general x1, matrix products, expert_apply(): jnp.dot(flattened, gate_w, preferred_element_type=jnp.float32)  5.49 us
    sub x2, other arithmetic, times(): return (a[0] * b[0] - a[1] * b[1], a[0] * b[1] + a[1] * b[0])  5.26 us
    dot_general x1, matrix products, mixer(): local = jnp.einsum('gks,gst->gkt', wide, kernel, precision=HIGHEST)  5.14 us
    dot_general x1, matrix products, mixer(): jnp.einsum('gkn,gtn->gkt', before, reads, precision=HIGHEST)  5.01 us

profile of v1, /device:TPU:15, one launch (start us, length us, event | category | flops | bytes accessed | tf_op | source)
XLA Modules:
  0.0 247.2 jit_solution(6646742588028251360)
XLA Ops:
  0.0 0.0 copy-start
  0.0 0.8 exp.65
  0.8 1.0 cosine_multiply_fusion
  1.8 1.0 fusion.90
  2.9 1.0 subtract_bitcast_fusion
  3.9 0.0 copy-start.8
  3.9 5.1 %multiply_subtract_fusion = (f32[16,16,16,64]{3,2,1,0:T(8,128)}, f32[16,16,16,64]{3,2,1,0:T(8,128)}, f32[16,16,16,64]{3,2,1,0:T(8,128)}, f32[16,16,16,64]{3,2,1,0:T(8,128)}) fusion(f32[16,16,64]{2,1,0:T(8,128)} %param.31, f32[16,16,64]{2,1,0:T(8,128)S(1)} %get-tuple-element.43, f32[16,16,64]{2,1,0:T(8,128)} %param.30, ...), kind=kLoop, calls=%fused_computation.18 | loop fusion | flops 3407872 | bytes 4718592 | tf_op jit(solution)/shard_map/sub | solution.py:109
  9.0 0.0 copy-done.8
  9.0 2.4 reshape.173
  11.4 3.3 %copy.54 = bf16[16,32,16,16]{1,3,2,0:T(8,128)(2,1)S(1)} copy(bf16[16,32,16,16]{3,0,2,1:T(8,128)(2,1)} %bitcast.93) | data formatting | bytes 524288 | tf_op jit(solution)/shard_map/transpose | solution.py:149
  14.7 3.9 %fusion.34 = f32[16,128,32]{1,2,0:T(8,128)S(1)} fusion(bf16[16,32,256]{1,2,0:T(8,128)(2,1)S(1)} %bitcast.87, f32[16,256,64]{2,1,0:T(8,128)} %bitcast.83, f32[16,256,64]{2,1,0:T(8,128)} %bitcast.85), kind=kOutput, calls=%fused_computation.44 | convolution fusion | flops 201850880 | bytes 2621440 | tf_op jit(solution)/shard_map/gks,gsn->gkn/dot_general | solution.py:154
  18.5 0.2 copy.71
  18.7 0.1 multiply_subtract_fusion.2
  18.9 0.1 subtract_add_fusion.2
  19.1 0.1 subtract_add_fusion.1
  19.2 0.1 fusion.54
  19.4 0.1 fusion.58
  19.5 0.1 fusion.62
  19.6 0.7 slice.116
  20.3 0.7 pad_maximum_fusion.7.block_ref
  20.9 6.2 %shard_map.217 = f32[8,16,128]{2,1,0:T(8,128)} custom-call(f32[16,128]{1,0:T(8,128)} %pad_maximum_fusion.7.block_ref), custom_call_target="tpu_custom_call" | custom-call | tf_op jit(solution)/shard_map/pallas_call | solution.py:59
  27.2 0.0 copy-start.1
  27.2 1.4 subtract_reduce_fusion
  28.6 2.3 subtract_add_fusion
  30.9 0.1 pad_maximum_fusion.6
  31.1 0.0 copy-done.1
  31.1 0.0 copy-start.2
  31.1 0.0 copy-start.3
  31.1 5.0 %fusion.32 = f32[16,32,256]{2,1,0:T(8,128)} fusion(f32[16,256,64]{2,1,0:T(8,128)} %bitcast.81, f32[16,256,64]{2,1,0:T(8,128)S(1)} %bitcast.79, f32[16,32,128]{2,0,1:T(8,128)S(1)} %pad_maximum_fusion.6), kind=kOutput, calls=%fused_computation.42 | convolution fusion | flops 201850880 | bytes 2883584 | tf_op jit(solution)/shard_map/gkn,gtn->gkt/dot_general | solution.py:191
  36.1 0.0 copy-done.2
  36.1 0.0 copy-done.3
  36.1 7.7 %fusion.33 = f32[16,256,256]{2,1,0:T(8,128)} fusion(f32[16,256,64]{2,1,0:T(8,128)S(1)} %bitcast.82, f32[16,256,64]{2,1,0:T(8,128)S(1)} %bitcast.80, f32[16,256,64]{2,1,0:T(8,128)S(1)} %bitcast.84, f32[16,256,64]{2,1,0:T(8,128)} %bitcast.86), kind=kOutput, calls=%fused_computation.43 | convolution fusion | flops 1611661312 | bytes 8388608 | tf_op jit(solution)/shard_map/gsn,gtn->gst/dot_general | solution.py:145
  43.9 0.7 broadcast_compare_fusion
  44.6 0.3 copy.59
  44.9 0.0 copy-done.10
  45.0 0.1 mul.908
  45.1 5.1 %fusion.44 = bf16[16,32,256]{2,1,0:T(8,128)(2,1)} fusion(f32[16,32,256]{2,1,0:T(8,128)} %fusion.32, bf16[16,32,256]{1,2,0:T(8,128)(2,1)S(1)} %bitcast.89, f32[16,256,256]{2,1,0:T(8,128)} %fusion.33, pred[256,256]{1,0:T(8,128)(4,1)} %broadcast_compare_fusion, bf16[16,32,256]{2,1,0:T(8,128)(2,1)S(1)} %copy.59, f32[16,256]{1,0:T(8,128)S(1)} %mul.908), kind=kOutput, calls=%fused_computation.52 | convolution fusion | flops 405405696 | bytes 5586944 | tf_op jit(solution)/shard_map/gks,gst->gkt/dot_general | solution.py:153
  50.2 1.4 copy.60
  51.6 4.2 %copy.61 = bf16[32,16,16,16]{3,2,1,0:T(8,128)(2,1)} copy(bf16[32,16,16,16]{0,3,1,2:T(8,128)(2,1)S(1)} %bitcast.94) | data formatting | bytes 524288 | tf_op jit(solution)/shard_map/transpose | solution.py:196
  55.8 3.9 %reshape_reshape.3.block_ref = bf16[4,128,256]{2,1,0:T(8,128)(2,1)} reshape(bf16[32,16,16,16]{3,2,1,0:T(8,128)(2,1)} %copy.61) | data formatting | bytes 524288 | tf_op jit(solution)/shard_map/reshape;reshape | solution.py:259
  59.7 7.0 %shard_map.218 = bf16[4,128,256]{2,1,0:T(8,128)(2,1)} custom-call(bf16[4,128,256]{2,1,0:T(8,128)(2,1)} %reshape_reshape.3.block_ref), custom_call_target="tpu_custom_call" | custom-call | tf_op jit(solution)/shard_map/pallas_call | solution.py:59
  66.7 1.1 copy.62
  67.9 0.1 copy.63
  68.0 0.0 copy-done.14
  68.0 0.0 copy-start.5
  68.0 0.0 copy-start.12
  68.1 2.4 multiply_reduce_fusion.1
  70.5 0.4 copy-done.5
  70.9 2.2 multiply_reduce_fusion
  73.0 0.5 fusion.113
  73.6 0.0 copy-start.11
  73.6 4.1 %convolution_add_fusion.2 = f32[128,2048]{1,0:T(8,128)} fusion(f32[128,2048]{1,0:T(8,128)S(1)} %get-tuple-element.60, bf16[512,2048]{1,0:T(8,128)(2,1)} %param.45, bf16[2048,512]{1,0:T(8,128)(2,1)} %param.44, f32[128,512]{1,0:T(8,128)S(1)} %fusion.113, f32[2048]{0:T(1024)S(1)} %copy-done.9, f32[128]{0:T(128)S(1)} %add_rsqrt_fusion), kind=kOutput, calls=%fused_computation.6 | convolution fusion | flops 538312704 | bytes 6562304 | tf_op jit(solution)/shard_map/dot_general | solution.py:272
  77.7 0.1 copy.64
  77.8 0.1 eq.75
  78.0 0.3 fusion.28
  78.2 0.1 convert_element_type.91
  78.4 0.1 copy.65
  78.4 2.9 %convolution_convert_fusion.1 = bf16[768,2048]{1,0:T(8,128)(2,1)} fusion(s32[128]{0:T(128)S(1)} %get-tuple-element.54, s32[128]{0:T(128)S(1)} %get-tuple-element.55, s32[128]{0:T(128)S(1)} %get-tuple-element.56, s32[128]{0:T(128)S(1)} %get-tuple-element.53, f32[128,2048]{1,0:T(8,128)S(1)} %get-tuple-element.60, f32[2048]{0:T(1024)S(1)} %copy-done.9, ...), kind=kOutput, calls=%fused_computation.3 | convolution fusion | flops 405700608 | bytes 4205056 | tf_op jit(solution)/shard_map/dot_general | solution.py:287
  81.3 73.2 %shard_map.219 = bf16[32,24,2048]{2,1,0:T(8,128)(2,1)} custom-call(bf16[32,24,2048]{2,1,0:T(8,128)(2,1)} %bitcast.92), custom_call_target="tpu_custom_call" | custom-call | tf_op jit(solution)/shard_map/pallas_call | solution.py:59
  154.5 5.5 %fusion.6 = f32[768,512]{1,0:T(8,128)} fusion(bf16[768,2048]{1,0:T(8,128)(2,1)} %bitcast.95, bf16[1,2048,512]{2,1,0:T(8,128)(2,1)} %param.40), kind=kOutput, calls=%fused_computation.14 | convolution fusion | flops 1610612736 | bytes 6815744 | tf_op jit(solution)/shard_map/dot_general | solution.py:215
  160.0 8.2 %convolution_convert_fusion = bf16[768,2048]{1,0:T(8,128)(2,1)} fusion(bf16[1,512,2048]{2,1,0:T(8,128)(2,1)S(1)} %copy-done, f32[768,512]{1,0:T(8,128)} %fusion.6, bf16[768,2048]{1,0:T(8,128)(2,1)} %bitcast.96, bf16[1,2048,512]{2,1,0:T(8,128)(2,1)} %param.41), kind=kOutput, calls=%fused_computation.2 | convolution fusion | flops 3225157632 | bytes 12058624 | tf_op jit(solution)/shard_map/dot_general | solution.py:218
  168.2 74.6 %shard_map.220 = bf16[32,24,2048]{2,1,0:T(8,128)(2,1)} custom-call(bf16[32,24,2048]{2,1,0:T(8,128)(2,1)} %bitcast.97), custom_call_target="tpu_custom_call" | custom-call | tf_op jit(solution)/shard_map/pallas_call | solution.py:59
  242.8 2.8 %convolution_add_fusion.1 = f32[128,2048]{1,0:T(8,128)S(1)} fusion(f32[128,2048]{1,0:T(8,128)S(1)} %copy-done.6, bf16[768,2048]{1,0:T(8,128)(2,1)} %bitcast.90, f32[128]{0:T(128)S(1)} %get-tuple-element.51, s32[128]{0:T(128)S(1)} %get-tuple-element.54, f32[128]{0:T(128)S(1)} %get-tuple-element.52, s32[128]{0:T(128)S(1)} %get-tuple-element.55, ...), kind=kOutput, calls=%fused_computation.5 | convolution fusion | flops 404094976 | bytes 5246976 | tf_op jit(solution)/shard_map/dot_general | solution.py:308
  245.6 1.6 fusion.2
  (41 shorter events, 0.3 us)
Async XLA Ops:
  0.0 160.0 %copy-start = (bf16[1,512,2048]{2,1,0:T(8,128)(2,1)S(1)}, bf16[1,512,2048]{2,1,0:T(8,128)(2,1)}, u32[]{:S(2)}) copy-start(bf16[1,512,2048]{2,1,0:T(8,128)(2,1)} %param.42) | copy-start | bytes 6291460
  3.9 5.1 %copy-start.8 = (bf16[512,256]{1,0:T(8,128)(2,1)S(1)}, bf16[512,256]{1,0:T(8,128)(2,1)}, u32[]{:S(2)}) copy-start(bf16[512,256]{1,0:T(8,128)(2,1)} %param.23) | copy-start | bytes 786436
  27.2 3.9 %copy-start.1 = (f32[16,16,16,64]{3,2,1,0:T(8,128)S(1)}, f32[16,16,16,64]{3,2,1,0:T(8,128)}, u32[]{:S(2)}) copy-start(f32[16,16,16,64]{3,2,1,0:T(8,128)} %get-tuple-element.11) | copy-start | bytes 3145732
  31.1 5.0 %copy-start.2 = (f32[16,16,16,64]{3,2,1,0:T(8,128)S(1)}, f32[16,16,16,64]{3,2,1,0:T(8,128)}, u32[]{:S(2)}) copy-start(f32[16,16,16,64]{3,2,1,0:T(8,128)} %get-tuple-element.12) | copy-start | bytes 3145732
  31.1 5.0 %copy-start.3 = (f32[16,16,16,64]{3,2,1,0:T(8,128)S(1)}, f32[16,16,16,64]{3,2,1,0:T(8,128)}, u32[]{:S(2)}) copy-start(f32[16,16,16,64]{3,2,1,0:T(8,128)} %get-tuple-element.61) | copy-start | bytes 3145732
  36.1 8.8 %copy-start.10 = (f32[16,16]{1,0:T(8,128)S(1)}, f32[16,16]{1,0:T(8,128)}, u32[]{:S(2)}) copy-start(f32[16,16]{1,0:T(8,128)} %param.32) | copy-start | bytes 3076
  55.8 12.2 %copy-start.14 = (f32[1024]{0:T(1024)S(1)}, f32[1024]{0:T(1024)}, u32[]{:S(2)}) copy-start(f32[1024]{0:T(1024)} %param.34) | copy-start | bytes 12292
  68.0 2.8 %copy-start.5 = (bf16[1024,2048]{1,0:T(8,128)(2,1)S(1)}, bf16[1024,2048]{1,0:T(8,128)(2,1)}, u32[]{:S(2)}) copy-start(bf16[1024,2048]{1,0:T(8,128)(2,1)} %param.36) | copy-start | bytes 12582916
  68.0 2.8 %copy-start.12 = (f32[1024]{0:T(1024)S(1)}, f32[1024]{0:T(1024)}, u32[]{:S(2)}) copy-start(f32[1024]{0:T(1024)} %param.35) | copy-start | bytes 12292
  70.9 2.2 copy-start.7
  70.9 2.2 copy-start.9
  73.6 4.2 %copy-start.11 = (s32[128,4]{0,1:T(4,128)S(1)}, s32[128,4]{0,1:T(4,128)}, u32[]{:S(2)}) copy-start(s32[128,4]{0,1:T(4,128)} %param.38) | copy-start | bytes 6148
  168.2 74.6 %copy-start.13 = (f32[128,4]{0,1:T(4,128)S(1)}, f32[128,4]{0,1:T(4,128)}, u32[]{:S(2)}) copy-start(f32[128,4]{0,1:T(4,128)} %param.39) | copy-start | bytes 6148
  168.2 74.6 %copy-start.6 = (f32[128,2048]{1,0:T(8,128)S(1)}, f32[128,2048]{1,0:T(8,128)}, u32[]{:S(2)}) copy-start(f32[128,2048]{1,0:T(8,128)} %convolution_add_fusion.2) | copy-start | bytes 3145732
  242.8 2.9 %copy-start.4 = (bf16[32,24,2048]{2,1,0:T(8,128)(2,1)S(1)}, bf16[32,24,2048]{2,1,0:T(8,128)(2,1)}, u32[]{:S(2)}) copy-start(bf16[32,24,2048]{2,1,0:T(8,128)(2,1)} %shard_map.220) | copy-start | bytes 9437188
